TPU v7x, 32 devices: a whole 2x2x4 slice. The times are simulated.
32 devices in a mesh: sp: 4 (over z), fs: 4 (over y, x), tp: 2 (over core).
Axes of the slice: x: 2, y: 2, z: 4, core: 2. Of those that a mesh axis runs over, the one named last changes fastest.
Arguments:
- tokens: bfloat16 [2048, 2048], P(('fs', 'sp')), parts along dimension 0, may hold values from -6 to 6
- norm_gain: bfloat16 [2048], replicated, may hold values from 0.099609375 to 1.8984375
- query_down: bfloat16 [2048, 512], P('sp'), may hold values from -0.125 to 0.125
- query_gain: bfloat16 [512], replicated, may hold values from 0.099609375 to 1.8984375
- latent_down: bfloat16 [2048, 256], replicated, may hold values from -0.125 to 0.125
- latent_gain: bfloat16 [256], replicated, may hold values from 0.099609375 to 1.8984375
- rope_down: bfloat16 [2048, 64], replicated, may hold values from -30 to 30
- query_up: bfloat16 [512, 1536], P(None, 'tp'), may hold values from -0.25 to 0.25
- key_up: bfloat16 [256, 1024], P(None, 'tp'), may hold values from -0.75 to 0.75
- value_up: bfloat16 [256, 1024], P(None, 'tp'), may hold values from -0.375 to 0.375
- glu_value: bfloat16 [2048, 1024], P('sp', 'tp'), may hold values from -0.125 to 0.125
- glu_gate: bfloat16 [2048, 1024], P('sp', 'tp'), may hold values from -0.125 to 0.125
- conv_taps: bfloat16 [31, 1024], P(None, 'tp'), may hold values from -1 to 1
- group_gain: bfloat16 [1024], P('tp'), may hold values from 0.099609375 to 1.8984375
- head_proj: bfloat16 [1024, 2048], P('tp', 'sp'), may hold values from -0.75 to 0.75
- channel_proj: bfloat16 [1024, 2048], P('tp', 'sp'), may hold values from -0.1875 to 0.1875
Outputs:
- mixed_out: bfloat16 [2048, 2048], P(('fs', 'sp'), 'tp'), parts along dimension 0
- log_weight: float32 [8, 2048], P('tp', ('fs', 'sp')), parts along dimension 1
There are 4 independent parts, one for each index of `fs`. A program takes and returns all parts, laid end to end along the dimension named above; an argument that names none is the same for every part. Nothing has to cross between parts.
All inputs are finite; a program needn't handle non-finite values.
Results may differ from a plain program's by a relative error of at most 0.015.
The roundings to bfloat16 on the way count: a program that leaves them out, or rounds other values in their place, can miss the bound.
Values may be sent and summed in bfloat16 or wider, within the bound.
A program may use at most 128 MiB of HBM per device.

v0:
```python
import jax
import jax.numpy as jnp
from jax import lax
from jax.sharding import PartitionSpec as P

NOPE = 128
ROPE = 64
VDIM = 128
KVR = 256
CH = 1024
GROUPS = 8
GRID_W = 64


norm_eps = 1e-06
rope_base = 10000.0
far_below = -1e30


def padded_2(block, sides, width):
    for axis, dim in sides:
        count = lax.axis_size(axis)
        forward = [(i, i + 1) for i in range(count - 1)]
        backward = [(target, source) for source, target in forward]
        low = lax.ppermute(
            lax.slice_in_dim(block, block.shape[dim] - width, None, axis=dim), axis, forward
        )
        high = lax.ppermute(lax.slice_in_dim(block, 0, width, axis=dim), axis, backward)
        block = jnp.concatenate([low, block, high], axis=dim)
    return block


def rms_scale(values, scale_gain):
    inv_rms = lax.rsqrt(jnp.mean(values * values, axis=-1, keepdims=True) + norm_eps)
    return values * inv_rms * scale_gain.astype(jnp.float32)


def angles_for(positions, rope_size):
    quarter = rope_size // 4
    inverse = rope_base ** (-jnp.arange(quarter, dtype=jnp.float32) / quarter)
    grid_row = (positions // GRID_W).astype(jnp.float32)
    grid_col = (positions % GRID_W).astype(jnp.float32)
    return jnp.concatenate([grid_row[:, None] * inverse, grid_col[:, None] * inverse], axis=-1)


def rotate(values, angles):
    half_size = values.shape[-1] // 2
    front_half = values[..., :half_size]
    back_half = values[..., half_size:]
    cosine = jnp.cos(angles)
    sine_part = jnp.sin(angles)
    return jnp.concatenate(
        [front_half * cosine - back_half * sine_part, back_half * cosine + front_half * sine_part],
        axis=-1,
    )


def key_block(normed, latent_down, latent_gain, rope_down, positions):
    latent = jnp.dot(normed, latent_down, preferred_element_type=jnp.float32)
    latent = rms_scale(latent, latent_gain).astype(jnp.bfloat16)
    rope_key = jnp.dot(normed, rope_down, preferred_element_type=jnp.float32)
    rope_key = rotate(rope_key, angles_for(positions, rope_key.shape[-1])).astype(jnp.bfloat16)
    return jnp.concatenate([latent, rope_key], axis=1)


def per_device(
    tokens,
    norm_gain,
    query_down,
    query_gain,
    latent_down,
    latent_gain,
    rope_down,
    query_up,
    key_up,
    value_up,
    glu_value,
    glu_gate,
    conv_taps,
    group_gain,
    head_proj,
    channel_proj,
):
    tok_count = tokens.shape[0]
    reach_rows = conv_taps.shape[0] // 2
    head_count = key_up.shape[1] // NOPE
    normed = rms_scale(tokens.astype(jnp.float32), norm_gain).astype(jnp.bfloat16)
    offsets = lax.axis_index("sp") * tok_count + jnp.arange(tok_count, dtype=jnp.int32)
    query_latent = jnp.dot(
        normed,
        lax.all_gather(query_down, "sp", axis=0, tiled=True),
        preferred_element_type=jnp.float32,
    )
    value_in = jnp.dot(
        normed,
        lax.all_gather(glu_value, "sp", axis=0, tiled=True),
        preferred_element_type=jnp.float32,
    )
    gate_in = jnp.dot(
        normed,
        lax.all_gather(glu_gate, "sp", axis=0, tiled=True),
        preferred_element_type=jnp.float32,
    )
    latent_query = rms_scale(query_latent, query_gain).astype(jnp.bfloat16)
    query_all = jnp.dot(latent_query, query_up, preferred_element_type=jnp.float32).reshape(
        tok_count, head_count, NOPE + ROPE
    )
    query_plain = query_all[:, :, :NOPE].astype(jnp.bfloat16)
    query_rope = rotate(query_all[:, :, NOPE:], angles_for(offsets, ROPE)[:, None, :]).astype(
        jnp.bfloat16
    )
    absorbed = jnp.einsum(
        "thd,rhd->htr",
        query_plain,
        key_up.reshape(KVR, head_count, NOPE),
        preferred_element_type=jnp.float32,
    ).astype(jnp.bfloat16)
    queries = jnp.concatenate([absorbed, jnp.transpose(query_rope, (1, 0, 2))], axis=-1)
    score_scale = (NOPE + ROPE) ** (-0.5)
    half_rows = tok_count // lax.axis_size("tp")
    first_row = lax.axis_index("tp") * half_rows
    own_rows = lax.dynamic_slice_in_dim(normed, first_row, half_rows, 0)
    own_positions = lax.dynamic_slice_in_dim(offsets, first_row, half_rows, 0)
    own_keys = key_block(own_rows, latent_down, latent_gain, rope_down, own_positions)
    block_keys = lax.all_gather(own_keys, ("sp", "tp"), axis=0, tiled=True)
    row_max = jnp.full((head_count, tok_count), far_below, jnp.float32)
    scores = (
        jnp.einsum("hqc,kc->hqk", queries, block_keys, preferred_element_type=jnp.float32)
        * score_scale
    )
    new_max = jnp.maximum(row_max, jnp.max(scores, axis=2))
    weights = jnp.exp(scores - new_max[:, :, None])
    new_sum = jnp.sum(weights, axis=2)
    added = jnp.einsum(
        "hqk,kr->hqr",
        weights.astype(jnp.bfloat16),
        block_keys[:, :KVR],
        preferred_element_type=jnp.float32,
    )
    gated_rows = (value_in * jax.nn.sigmoid(gate_in)).astype(jnp.bfloat16)
    padded = padded_2(gated_rows, (("sp", 0),), reach_rows)
    filtered = padded[0:tok_count].astype(jnp.float32) * conv_taps[0].astype(jnp.float32)
    for tap_index in range(1, conv_taps.shape[0]):
        filtered = filtered + padded[tap_index : tap_index + tok_count].astype(
            jnp.float32
        ) * conv_taps[tap_index].astype(jnp.float32)
    grouped = filtered.reshape(tok_count, -1, CH // GROUPS)
    centred = grouped - jnp.mean(grouped, axis=-1, keepdims=True)
    spread = jnp.mean(centred * centred, axis=-1, keepdims=True)
    normal_groups = (centred * lax.rsqrt(spread + norm_eps)).reshape(tok_count, -1)
    conv_branch = jax.nn.silu(normal_groups * group_gain.astype(jnp.float32)).astype(jnp.bfloat16)
    attended = (added / new_sum[:, :, None]).astype(jnp.bfloat16)
    log_weight = new_max + jnp.log(new_sum)
    head_out = jnp.einsum(
        "htr,rhv->thv",
        attended,
        value_up.reshape(KVR, head_count, VDIM),
        preferred_element_type=jnp.float32,
    )
    head_out = head_out.reshape(tok_count, head_count * VDIM).astype(jnp.bfloat16)
    mixed_in = jnp.concatenate([head_out, conv_branch], axis=1)
    out_weight = jnp.concatenate([head_proj, channel_proj], axis=0)
    partial_terms = jnp.dot(
        mixed_in,
        lax.all_gather(out_weight, "sp", axis=1, tiled=True),
        preferred_element_type=jnp.float32,
    )
    mixed_out = lax.psum_scatter(
        partial_terms.astype(jnp.bfloat16), "tp", scatter_dimension=1, tiled=True
    )
    return (mixed_out, log_weight)


def solution(mesh):
    in_specs = (
        P(("fs", "sp"), None),
        P(),
        P("sp", None),
        P(),
        P(),
        P(),
        P(),
        P(None, "tp"),
        P(None, "tp"),
        P(None, "tp"),
        P("sp", "tp"),
        P("sp", "tp"),
        P(None, "tp"),
        P("tp"),
        P("tp", "sp"),
        P("tp", "sp"),
    )
    out_specs = (P(("fs", "sp"), "tp"), P("tp", ("fs", "sp")))
    return jax.shard_map(
        per_device, mesh=mesh, in_specs=in_specs, out_specs=out_specs, check_vma=False
    )
```

profile of v0, /device:TPU:0, one launch (start us, length us, event | category | flops | bytes accessed | tf_op | source)
XLA Modules:
  0.0 250.3 jit_solution(11534112967681167767)
XLA Ops:
  7.2 0.7 all-gather.7.cloned.1.call-update
  8.0 0.7 all-gather.9.cloned.1.call-update
  8.7 0.7 all-gather.5.cloned.1.call-update
  9.5 2.2 pad_maximum_fusion
  12.4 0.4 multiply_reduce_fusion.2
  13.2 0.6 convert_element_type.278
  14.0 0.2 fusion.26
  14.6 17.5 %all_gather.16 = bf16[512,320]{1,0:T(8,128)(2,1)S(1)} all-gather(bf16[64,320]{1,0:T(8,128)(2,1)S(1)} %pad_maximum_fusion.3), channel_id=1, replica_groups=mesh['sp'=4,'fs'=4,'tp'=2] {'sp','tp'}, dimensions={0}, use_global_device_ids=true | all-gather | bytes 368640 | tf_op jit(solution)/shard_map/all_gather | solution.py:125
  32.0 0.6 slice_convert_fusion.31
  32.7 0.7 slice_convert_fusion.32
  33.4 26.5 %all-gather.7.cloned.1.call-done = bf16[2048,512]{1,0:T(8,128)(2,1)} async-done(((bf16[512,512]{1,0:T(8,128)(2,1)}), bf16[2048,512]{1,0:T(8,128)(2,1)}) %all-gather.7.cloned.1.call-update) | async-done | bytes 2097168 | tf_op jit(solution)/shard_map/all_gather | solution.py:96
  59.8 2.0 fusion.75
  61.9 44.5 %all-gather.9.cloned.1.call-done = bf16[2048,512]{1,0:T(8,128)(2,1)} async-done(((bf16[512,512]{1,0:T(8,128)(2,1)}), bf16[2048,512]{1,0:T(8,128)(2,1)}) %all-gather.9.cloned.1.call-update) | async-done | bytes 2097168 | tf_op jit(solution)/shard_map/all_gather | solution.py:101
  106.4 2.1 fusion.6
  108.5 0.6 copy-done.6
  109.1 0.6 fusion.73
  109.7 2.7 %collective-permute-start = (bf16[15,512]{1,0:T(8,128)(2,1)}, bf16[15,512]{1,0:T(8,128)(2,1)}, u32[]{:S(2)}, u32[]{:S(2)}) collective-permute-start(bf16[15,512]{1,0:T(8,128)(2,1)} %get-tuple-element.6), channel_id=1, source_target_pairs={{0,8},{8,16},{16,24},{1,9},{9,17},{17,25},{2,10},{10,18},{18,26},{... | collective-permute-start | bytes 46088 | tf_op jit(solution)/shard_map/ppermute | solution.py:25
  112.4 1.3 collective-permute-start.1
  113.7 38.9 %all-gather.5.cloned.1.call-done = bf16[2048,512]{1,0:T(8,128)(2,1)} async-done(((bf16[512,512]{1,0:T(8,128)(2,1)}), bf16[2048,512]{1,0:T(8,128)(2,1)}) %all-gather.5.cloned.1.call-update) | async-done | bytes 2097168 | tf_op jit(solution)/shard_map/all_gather | solution.py:91
  152.6 2.1 multiply_reduce_fusion.1
  154.8 0.5 fusion.30
  155.3 0.3 convolution_convert_fusion.1
  155.6 0.6 fusion.74
  156.2 0.3 fusion.11
  156.8 0.6 fusion.7
  157.9 2.3 multiply_add_fusion
  160.3 0.2 reduce_sum.58
  160.5 0.4 multiply_reduce_fusion
  161.4 72.0 %all-gather.11.cloned.1.call-done = bf16[1024,2048]{1,0:T(8,128)(2,1)} async-done(((bf16[1024,512]{1,0:T(8,128)(2,1)}), bf16[1024,2048]{1,0:T(8,128)(2,1)}) %all-gather.11.cloned.1.call-update) | async-done | bytes 4194320 | tf_op jit(solution)/shard_map/all_gather | solution.py:165
  233.4 3.7 %convolution_convert_fusion = bf16[128,2048]{1,0:T(8,128)(2,1)} fusion(bf16[1024,2048]{1,0:T(8,128)(2,1)} %all-gather.11.cloned.1.call-done, bf16[128,512]{1,0:T(8,128)(2,1)S(1)} %multiply_convert_fusion, bf16[128,512]{1,0:T(8,128)(2,1)S(1)} %copy.28), kind=kOutput, calls=%fused_computation | convolution fusion | flops 537657344 | bytes 4980736 | tf_op jit(solution)/shard_map/dot_general | solution.py:163
  237.2 0.6 log_add_fusion
  237.8 6.0 %reduce-scatter.2.cloned.1.call-done = bf16[128,1024]{1,0:T(8,128)(2,1)} async-done(((bf16[128,2048]{1,0:T(8,128)(2,1)}), bf16[128,1024]{1,0:T(8,128)(2,1)}) %reduce-scatter.2.cloned.1.call-update) | async-done | bytes 262160 | tf_op jit(solution)/shard_map/reduce_scatter | solution.py:168
  (129 shorter events, 2.6 us)
Async XLA Ops:
  7.2 5.2 %copy-start = (bf16[2048,256]{1,0:T(8,128)(2,1)S(1)}, bf16[2048,256]{1,0:T(8,128)(2,1)}, u32[]{:S(2)}) copy-start(bf16[2048,256]{1,0:T(8,128)(2,1)} %param.20) | copy-start | bytes 3145732
  7.2 52.6 %all-gather.7.cloned.1.call-start = ((), (), s32[]{:S(2)}) async-start(), calls=%async_computation.2 | async-start | bytes 2621440 | tf_op jit(solution)/shard_map/all_gather | solution.py:96
  7.9 4.0 %copy-start.41 = (bf16[2048]{0:T(1024)(128)(2,1)S(1)}, bf16[2048]{0:T(1024)(128)(2,1)}, u32[]{:S(2)}) copy-start(bf16[2048]{0:T(1024)(128)(2,1)} %param.17) | copy-start | bytes 12292
  7.9 4.0 %copy-start.1 = (bf16[128,2048]{1,0:T(8,128)(2,1)S(1)}, bf16[128,2048]{1,0:T(8,128)(2,1)}, u32[]{:S(2)}) copy-start(bf16[128,2048]{1,0:T(8,128)(2,1)} %param.16) | copy-start | bytes 1572868
  7.9 98.4 %all-gather.9.cloned.1.call-start = ((), (), s32[]{:S(2)}) async-start(), calls=%async_computation.3 | async-start | bytes 2621440 | tf_op jit(solution)/shard_map/all_gather | solution.py:101
  8.7 143.9 %all-gather.5.cloned.1.call-start = ((), (), s32[]{:S(2)}) async-start(), calls=%async_computation.1 | async-start | bytes 2621440 | tf_op jit(solution)/shard_map/all_gather | solution.py:91
  9.4 224.0 %all-gather.11.cloned.1.call-start = ((), (), s32[]{:S(2)}) async-start(), calls=%async_computation.4 | async-start | bytes 5242880 | tf_op jit(solution)/shard_map/all_gather | solution.py:165
  11.7 1.2 copy-start.44
  11.7 1.2 copy-start.42
  11.7 1.2 copy-start.4
  11.7 1.4 copy-start.5
  11.7 1.5 copy-start.43
  11.7 232.0 %reduce-scatter.2.cloned.1.call-start = ((), (), s32[]{:S(2)}) async-start(), calls=%async_computation.5 | async-start | bytes 786432 | tf_op jit(solution)/shard_map/reduce_scatter | solution.py:168
  11.9 2.1 copy-start.3
  12.4 19.7 %copy-start.8 = (bf16[31,512]{1,0:T(8,128)(2,1)S(1)}, bf16[31,512]{1,0:T(8,128)(2,1)}, u32[]{:S(2)}) copy-start(bf16[31,512]{1,0:T(8,128)(2,1)} %param.28) | copy-start | bytes 95236
  109.1 45.6 %copy-start.2 = (bf16[512,768]{1,0:T(8,128)(2,1)S(1)}, bf16[512,768]{1,0:T(8,128)(2,1)}, u32[]{:S(2)}) copy-start(bf16[512,768]{1,0:T(8,128)(2,1)} %param.23) | copy-start | bytes 2359300
  109.7 47.8 %collective-permute-start = (bf16[15,512]{1,0:T(8,128)(2,1)}, bf16[15,512]{1,0:T(8,128)(2,1)}, u32[]{:S(2)}, u32[]{:S(2)}) collective-permute-start(bf16[15,512]{1,0:T(8,128)(2,1)} %get-tuple-element.6), channel_id=1, source_target_pairs={{0,8},{8,16},{16,24},{1,9},{9,17},{17,25},{2,10},{10,18},{18,26},{... | collective-permute-start | bytes 46088 | tf_op jit(solution)/shard_map/ppermute | solution.py:25
  112.4 45.1 %collective-permute-start.1 = (bf16[15,512]{1,0:T(8,128)(2,1)}, bf16[15,512]{1,0:T(8,128)(2,1)}, u32[]{:S(2)}, u32[]{:S(2)}) collective-permute-start(bf16[15,512]{1,0:T(8,128)(2,1)} %get-tuple-element.7), channel_id=1, source_target_pairs={{8,0},{16,8},{24,16},{9,1},{17,9},{25,17},{10,2},{18,10},{26,18},{... | collective-permute-start | bytes 46088 | tf_op jit(solution)/shard_map/ppermute | solution.py:28
  156.5 1.0 copy-start.7
  156.5 1.0 copy-start.9
  156.5 1.0 copy-start.10
  156.5 1.0 copy-start.11
  156.5 1.0 copy-start.12
  156.6 1.0 copy-start.13
  156.6 1.0 copy-start.14
  156.6 1.0 copy-start.15
  156.6 1.0 copy-start.16
  156.6 1.0 copy-start.17
  156.6 1.0 copy-start.18
  156.6 1.0 copy-start.19
  156.6 1.0 copy-start.20
  157.4 3.9 %copy-start.40 = (f32[512]{0:T(512)S(1)}, f32[512]{0:T(512)}, u32[]{:S(2)}) copy-start(f32[512]{0:T(512)} %convert_element_type.278) | copy-start | bytes 6148
  (20 other events, 20.2 us)
Sparse Core Ops, SparseCore 0:
  9.6 50.2 all-gather.6
  61.4 44.9 all-gather.8
  107.9 44.6 all-gather.4
  154.0 79.3 all-gather.10
  237.3 6.3 reduce-scatter.1
where the time goes:
time: 251 us; the launch traced here: 250 us
  waiting for transfers between devices  190 us (76%)
  blocking collectives  17.5 us (7%)
  between operations  14.7 us (6%)
  matrix products  12.5 us (5%)
  other arithmetic  9.21 us (4%)
  starting transfers between devices  4.14 us (2%)
    all_gather x1, waiting for transfers between devices, per_device(): lax.all_gather(out_weight, 'sp', axis=1, tiled=True)  72 us
    all_gather x1, waiting for transfers between devices, per_device(): lax.all_gather(glu_gate, 'sp', axis=0, tiled=True)  44.5 us
    all_gather x1, waiting for transfers between devices, per_device(): lax.all_gather(query_down, 'sp', axis=0, tiled=True)  38.9 us
    all_gather x1, waiting for transfers between devices, per_device(): lax.all_gather(glu_value, 'sp', axis=0, tiled=True)  26.5 us
    all_gather x1, blocking collectives, per_device(): block_keys = lax.all_gather(own_keys, ('sp', 'tp'), axis=0, tiled=True)  17.5 us
    reduce_scatter x1, waiting for transfers between devices, per_device(): lax.psum_scatter(partial_terms.astype(jnp.bfloat16), 'tp', scatter_dimens...  5.98 us
  transfers between devices with their start and end apart: 7, of which 5 were waited for; matrix products, arithmetic and copies ran while one was open for 8% of the time, Pallas kernels for 0%

commit v1 on v0

--- a/solution.py
+++ b/solution.py
@@ -1,6 +1,11 @@
+import functools
+
 import jax
 import jax.numpy as jnp
+import numpy as np
 from jax import lax
+from jax.experimental import pallas as pl
+from jax.experimental.pallas import tpu as pltpu
 from jax.sharding import PartitionSpec as P
 
 NOPE = 128
@@ -171,6 +176,510 @@
     return (mixed_out, log_weight)
 
 
+LANES = 128
+MESH = pl.DeviceIdType.MESH
+F32 = jnp.float32
+BF16 = jnp.bfloat16
+Z_IN, X_IN, Y_IN, DX_IN, DY_IN = range(5)
+Z_LOW, Z_HIGH, Z_FWD, X_OUT, Y_OUT, DX_OUT, DY_OUT = range(7)
+
+
+def rope_tables(length):
+    quarter = ROPE // 4
+    inverse = np.float32(rope_base) ** (-np.arange(quarter, dtype=np.float32) / np.float32(quarter))
+    positions = np.arange(length)
+    row = (positions // GRID_W).astype(np.float32)[:, None] * inverse
+    col = (positions % GRID_W).astype(np.float32)[:, None] * inverse
+    angles = np.concatenate([row, col], axis=1).astype(np.float32)
+    cosine, sine = np.cos(angles), np.sin(angles)
+    tables = np.zeros((3, length, LANES), np.float32)
+    half = ROPE // 2
+    tables[0, :, :half] = cosine
+    tables[0, :, half:ROPE] = cosine
+    tables[1, :, :half] = -sine
+    tables[2, :, half:ROPE] = sine
+    return tables
+
+
+def dot(a, b):
+    return jnp.dot(a, b, preferred_element_type=F32)
+
+
+def dot_nt(a, b):
+    return lax.dot_general(a, b, (((1,), (1,)), ((), ())), preferred_element_type=F32)
+
+
+def fused_kernel(
+    n_sp,
+    tokens, norm_gain, query_down, query_gain, latent_down, latent_gain, rope_down, query_up,
+    key_up, value_up, glu_value, glu_gate, conv_taps, group_gain, head_proj, channel_proj, tables,
+    out, log_out,
+    w_q, w_g, w_o, tok_v, lat_v, rope_v, qup_v, kup_v, vup_v, tab_v,
+    normed, keys, key_tmp, q_acc, q_lat, q_scr, g_acc, mixed, gated, low_rows, high_rows, padded,
+    parts, peer_parts,
+    load_sem, recv_sem, send_sem, key_recv, key_send, pair_recv, pair_send, halo_recv, halo_send,
+):
+    z = lax.axis_index("sp")
+    c = lax.axis_index("fs")
+    t = lax.axis_index("tp")
+    peer = 1 - t
+    c_x = c + 1 - 2 * (c % 2)
+    c_y = (c + 2) % 4
+    c_d = 3 - c
+    rows = tokens.shape[0]
+    depth = query_down.shape[0]
+    q_cols = w_q.shape[2]
+    chans = glu_value.shape[1]
+    heads = key_up.shape[1] // NOPE
+    head_rows = head_proj.shape[0]
+    out_rows = w_o.shape[1]
+
+    loads = {}
+
+    def load(name, src, dst):
+        copy = pltpu.make_async_copy(src, dst, load_sem.at[len(loads)])
+        copy.start()
+        loads[name] = copy
+
+    load("wq", query_down.at[:, pl.ds(pl.multiple_of(t * q_cols, LANES), q_cols)], w_q.at[z])
+    load("gv", glu_value, w_g.at[z, :, pl.ds(0, chans)])
+    load("gg", glu_gate, w_g.at[z, :, pl.ds(chans, chans)])
+    load("tok", tokens, tok_v)
+    load("lat", latent_down, lat_v)
+    load("rope", rope_down, rope_v)
+    load("tab", tables.at[:, pl.ds(pl.multiple_of(z * rows, LANES), rows), :], tab_v)
+    load("hp", head_proj, w_o.at[z, pl.ds(0, head_rows), :])
+    load("cp", channel_proj, w_o.at[z, pl.ds(head_rows, out_rows - head_rows), :])
+    load("qup", query_up, qup_v)
+    load("kup", key_up, kup_v)
+    load("vup", value_up, vup_v)
+
+    barrier = pltpu.get_barrier_semaphore()
+    partners = [{"sp": (z + d) % n_sp} for d in range(1, n_sp)]
+    partners += [{"fs": c_x}, {"fs": c_y}, {"tp": peer}]
+    for partner in partners:
+        pl.semaphore_signal(barrier, inc=1, device_id=partner, device_id_type=MESH)
+    pl.semaphore_wait(barrier, len(partners))
+
+    direct_rows = (out_rows // 4) // 64 * 64
+    units = [
+        (w_q, 0, depth, True),
+        (w_g, 0, depth, True),
+        (w_o, 0, out_rows - direct_rows, True),
+        (w_o, out_rows - direct_rows, direct_rows, False),
+    ]
+    Q, G, O, D = range(4)
+
+    def block(u, shard, quarter, half=None):
+        buf, first, count, shared = units[u]
+        if not shared:
+            return buf.at[shard, pl.ds(first, count), :]
+        size = count // 4
+        start = first + quarter * size
+        if half is not None:
+            size = size // 2
+            start = start + half * size
+        return buf.at[shard, pl.ds(pl.multiple_of(start, 16), size), :]
+
+    def remote(u, shard, ref, out_kind, in_kind, device):
+        return pltpu.make_async_remote_copy(
+            src_ref=ref, dst_ref=ref,
+            send_sem=send_sem.at[u, shard, out_kind], recv_sem=recv_sem.at[u, shard, in_kind],
+            device_id=device, device_id_type=MESH,
+        )
+
+    def own_copy(u, low):
+        return remote(
+            u, z, block(u, z, c), Z_LOW if low else Z_HIGH, Z_IN, {"sp": z - 1 if low else z + 1}
+        )
+
+    def send_own(u):
+        @pl.when(z > 0)
+        def _():
+            own_copy(u, True).start()
+
+        @pl.when(z < n_sp - 1)
+        def _():
+            own_copy(u, False).start()
+
+    nearest = jnp.minimum(z, n_sp - 1 - z)
+    arrivals = []
+    for k in range(n_sp - 1):
+        both = k < 2 * nearest
+        distance = jnp.where(both, k // 2 + 1, k - nearest + 1)
+        from_low = jnp.where(both, 1 - k % 2, (2 * z > n_sp - 1).astype(jnp.int32))
+        shard = z - distance * (2 * from_low - 1)
+        arrivals.append((shard, z + 2 * from_low - 1))
+
+    def forward_copy(u, k):
+        shard, target = arrivals[k]
+        return remote(u, shard, block(u, shard, c), Z_FWD, Z_IN, {"sp": target})
+
+    def when_forward(k, action):
+        target = arrivals[k][1]
+
+        @pl.when((target >= 0) & (target < n_sp))
+        def _():
+            action()
+
+    def side_copies(u, k):
+        shard, _ = arrivals[k]
+        mine = block(u, shard, c)
+        return (
+            remote(u, shard, mine, X_OUT, X_IN, {"fs": c_x}),
+            remote(u, shard, mine, Y_OUT, Y_IN, {"fs": c_y}),
+        )
+
+    def corner_copies(u, k):
+        shard, _ = arrivals[k]
+        return (
+            remote(u, shard, block(u, shard, c_x, 0), DY_OUT, DY_IN, {"fs": c_y}),
+            remote(u, shard, block(u, shard, c_y, 1), DX_OUT, DX_IN, {"fs": c_x}),
+        )
+
+    def wait_in(u, k, kind, quarter, half=None):
+        shard, _ = arrivals[k]
+        remote(u, shard, block(u, shard, quarter, half), Z_FWD, kind, {"fs": c_x}).wait_recv()
+
+    def step_a(u, k):
+        wait_in(u, k, Z_IN, c)
+        when_forward(k, lambda: forward_copy(u, k).start())
+        if units[u][3]:
+            for copy in side_copies(u, k):
+                copy.start()
+
+    def step_b(u, k):
+        to_y, to_x = corner_copies(u, k)
+        wait_in(u, k, X_IN, c_x)
+        to_y.start()
+        wait_in(u, k, Y_IN, c_y)
+        to_x.start()
+
+    def step_c(u, k):
+        wait_in(u, k, DY_IN, c_d, 0)
+        wait_in(u, k, DX_IN, c_d, 1)
+
+    loads["wq"].wait()
+    send_own(Q)
+    loads["gv"].wait()
+    loads["gg"].wait()
+    send_own(G)
+
+    loads["tok"].wait()
+    values = tok_v[...].astype(F32)
+    normed[...] = rms_scale(values, norm_gain[...]).astype(BF16)
+
+    def rotate_lanes(v):
+        half = ROPE // 2
+        return (
+            v * tab_v[0] + pltpu.roll(v, LANES - half, 1) * tab_v[1] + pltpu.roll(v, half, 1) * tab_v[2]
+        )
+
+    loads["lat"].wait()
+    latent = rms_scale(dot(normed[...], lat_v[...]), latent_gain[...])
+    keys[z, :, 0:KVR] = latent.astype(BF16)
+    loads["rope"].wait()
+    loads["tab"].wait()
+    key_tmp[...] = jnp.zeros_like(key_tmp)
+    key_tmp[:, 0:ROPE] = dot(normed[...], rope_v[...])
+    keys[z, :, KVR : KVR + LANES] = rotate_lanes(key_tmp[...]).astype(BF16)
+
+    def key_copy(d):
+        return pltpu.make_async_remote_copy(
+            src_ref=keys.at[z], dst_ref=keys.at[z],
+            send_sem=key_send.at[d], recv_sem=key_recv.at[d],
+            device_id={"sp": (z + d) % n_sp}, device_id_type=MESH,
+        )
+
+    def key_arrival(d):
+        source = (z + n_sp - d) % n_sp
+        return pltpu.make_async_remote_copy(
+            src_ref=keys.at[source], dst_ref=keys.at[source],
+            send_sem=key_send.at[d], recv_sem=key_recv.at[d],
+            device_id={"sp": source}, device_id_type=MESH,
+        )
+
+    for d in range(1, n_sp):
+        key_copy(d).start()
+
+    def add_shard(acc, weights, shard, first=False):
+        columns = pl.ds(pl.multiple_of(shard * depth, LANES), depth)
+        term = dot(normed[:, columns], weights[shard])
+        acc[...] = term if first else acc[...] + term
+
+    add_shard(q_acc, w_q, z, True)
+    add_shard(g_acc, w_g, z, True)
+
+    last = n_sp - 2
+    loads["hp"].wait()
+    loads["cp"].wait()
+    for k in range(last + 1):
+        step_a(Q, k)
+        if k:
+            step_b(Q, k - 1)
+        if k > 1:
+            step_c(Q, k - 2)
+            add_shard(q_acc, w_q, arrivals[k - 2][0])
+    send_own(O)
+    step_b(Q, last)
+    step_a(G, 0)
+    for k in range(max(last - 1, 0), last + 1):
+        step_c(Q, k)
+        add_shard(q_acc, w_q, arrivals[k][0])
+
+    q_lat[t] = q_acc[...]
+    q_copy = pltpu.make_async_remote_copy(
+        src_ref=q_lat.at[t], dst_ref=q_lat.at[t], send_sem=pair_send.at[0], recv_sem=pair_recv.at[0],
+        device_id={"tp": peer}, device_id_type=MESH,
+    )
+    q_copy.start()
+    loads["qup"].wait()
+    loads["kup"].wait()
+    loads["vup"].wait()
+    pltpu.make_async_remote_copy(
+        src_ref=q_lat.at[peer], dst_ref=q_lat.at[peer], send_sem=pair_send.at[0],
+        recv_sem=pair_recv.at[0], device_id={"tp": peer}, device_id_type=MESH,
+    ).wait_recv()
+    whole_q = jnp.concatenate([q_lat[0], q_lat[1]], axis=1)
+    latent_query = rms_scale(whole_q, query_gain[...]).astype(BF16)
+    q_scr[...] = dot(latent_query, qup_v[...])
+    for d in range(1, n_sp):
+        key_arrival(d).wait_recv()
+
+    def attend(h, shifted):
+        start = h * (NOPE + ROPE)
+        source = q_scr[...]
+        if start % LANES:
+            source, start = shifted, start - ROPE
+        plain = source[:, start : start + NOPE].astype(BF16)
+        rope_part = rotate_lanes(source[:, start + NOPE : start + NOPE + LANES]).astype(BF16)
+        absorbed = dot_nt(plain, kup_v[:, h * NOPE : (h + 1) * NOPE]).astype(BF16)
+        query = jnp.concatenate([absorbed, rope_part], axis=1)
+        all_keys = keys[...].reshape(n_sp * rows, KVR + LANES)
+        scores = dot_nt(query, all_keys) * (NOPE + ROPE) ** (-0.5)
+        row_max = jnp.max(scores, axis=1, keepdims=True)
+        weights = jnp.exp(scores - row_max)
+        total = jnp.sum(weights, axis=1, keepdims=True)
+        added = dot(weights.astype(BF16), all_keys[:, 0:KVR])
+        attended = (added / total).astype(BF16)
+        head_out = dot(attended, vup_v[:, h * VDIM : (h + 1) * VDIM])
+        mixed[:, h * VDIM : (h + 1) * VDIM] = head_out.astype(BF16)
+        return row_max + jnp.log(total)
+
+    whole = q_scr[...]
+    shifted = pltpu.roll(whole, whole.shape[1] - ROPE, 1)
+    lane = lax.broadcasted_iota(jnp.int32, (rows, LANES), 1)
+    logs = jnp.zeros((rows, LANES), F32)
+    relays = [lambda: step_a(G, 1), lambda: step_b(G, 0), lambda: step_a(G, 2), lambda: None]
+    if n_sp == 2:
+        relays = [lambda: step_b(G, 0)]
+    for h in range(heads):
+        logs = jnp.where(lane == h, attend(h, shifted), logs)
+        if h < len(relays):
+            relays[h]()
+    for h in range(heads, len(relays)):
+        relays[h]()
+    log_out[...] = jnp.transpose(logs)[0:heads, :]
+
+    send_own(D)
+    if n_sp > 2:
+        step_b(G, 1)
+        step_c(G, 0)
+        add_shard(g_acc, w_g, arrivals[0][0])
+        step_a(O, 0)
+        step_b(G, 2)
+        step_c(G, 1)
+        add_shard(g_acc, w_g, arrivals[1][0])
+        step_a(O, 1)
+        step_c(G, 2)
+        add_shard(g_acc, w_g, arrivals[2][0])
+    else:
+        step_a(O, 0)
+        step_c(G, 0)
+        add_shard(g_acc, w_g, arrivals[0][0])
+
+    halo = low_rows.shape[0]
+    reach = conv_taps.shape[0] // 2
+    gated[...] = (g_acc[:, 0:chans] * jax.nn.sigmoid(g_acc[:, chans : 2 * chans])).astype(BF16)
+    up_copy = pltpu.make_async_remote_copy(
+        src_ref=gated.at[pl.ds(rows - halo, halo), :], dst_ref=low_rows,
+        send_sem=halo_send.at[0], recv_sem=halo_recv.at[0],
+        device_id={"sp": z + 1}, device_id_type=MESH,
+    )
+    down_copy = pltpu.make_async_remote_copy(
+        src_ref=gated.at[pl.ds(0, halo), :], dst_ref=high_rows,
+        send_sem=halo_send.at[1], recv_sem=halo_recv.at[1],
+        device_id={"sp": z - 1}, device_id_type=MESH,
+    )
+
+    @pl.when(z < n_sp - 1)
+    def _():
+        up_copy.start()
+
+    @pl.when(z > 0)
+    def _():
+        down_copy.start()
+
+    padded[halo : halo + rows, :] = gated[...].astype(F32)
+    step_b(O, 0)
+    if n_sp > 2:
+        step_a(O, 2)
+
+    @pl.when(z > 0)
+    def _():
+        up_copy.wait_recv()
+        padded[0:halo, :] = low_rows[...].astype(F32)
+
+    @pl.when(z == 0)
+    def _():
+        padded[0:halo, :] = jnp.zeros((halo, chans), F32)
+
+    @pl.when(z < n_sp - 1)
+    def _():
+        down_copy.wait_recv()
+        padded[halo + rows : 2 * halo + rows, :] = high_rows[...].astype(F32)
+
+    @pl.when(z == n_sp - 1)
+    def _():
+        padded[halo + rows : 2 * halo + rows, :] = jnp.zeros((halo, chans), F32)
+
+    group = CH // GROUPS
+    for g in range(chans // group):
+        lanes = slice(g * group, (g + 1) * group)
+        taps = conv_taps[:, lanes].astype(F32)
+        filtered = jnp.zeros((rows, group), F32)
+        for j in range(conv_taps.shape[0]):
+            first = halo - reach + j
+            filtered = filtered + padded[first : first + rows, lanes] * taps[j : j + 1, :]
+        centred = filtered - jnp.mean(filtered, axis=1, keepdims=True)
+        spread = jnp.mean(centred * centred, axis=1, keepdims=True)
+        branch = centred * lax.rsqrt(spread + norm_eps) * group_gain[:, lanes].astype(F32)
+        branch = branch * jax.nn.sigmoid(branch)
+        mixed[:, heads * VDIM + g * group : heads * VDIM + (g + 1) * group] = branch.astype(BF16)
+        if g == 0 and n_sp > 2:
+            step_b(O, 1)
+        if g == 2:
+            step_c(O, 0)
+            step_a(D, 0)
+
+    def add_part(shard):
+        parts[shard] = dot(mixed[...], w_o[shard]).astype(BF16)
+
+    add_part(z)
+    if n_sp > 2:
+        step_a(D, 1)
+        add_part(arrivals[0][0])
+        step_b(O, 2)
+        step_c(O, 1)
+        step_a(D, 2)
+        add_part(arrivals[1][0])
+        step_c(O, 2)
+        add_part(arrivals[2][0])
+    else:
+        add_part(arrivals[0][0])
+
+    half_sp = n_sp // 2
+    p_copy = pltpu.make_async_remote_copy(
+        src_ref=parts.at[pl.ds(peer * half_sp, half_sp)], dst_ref=peer_parts,
+        send_sem=pair_send.at[1], recv_sem=pair_recv.at[1],
+        device_id={"tp": peer}, device_id_type=MESH,
+    )
+    p_copy.start()
+
+    for u in range(len(units)):
+        @pl.when(z > 0)
+        def _():
+            own_copy(u, True).wait_send()
+
+        @pl.when(z < n_sp - 1)
+        def _():
+            own_copy(u, False).wait_send()
+
+        for k in range(n_sp - 1):
+            when_forward(k, lambda: forward_copy(u, k).wait_send())
+            if units[u][3]:
+                for copy in side_copies(u, k) + corner_copies(u, k):
+                    copy.wait_send()
+    for d in range(1, n_sp):
+        key_copy(d).wait_send()
+    q_copy.wait_send()
+
+    @pl.when(z < n_sp - 1)
+    def _():
+        up_copy.wait_send()
+
+    @pl.when(z > 0)
+    def _():
+        down_copy.wait_send()
+
+    p_copy.wait()
+    width = parts.shape[2]
+    for i in range(half_sp):
+        total = parts[t * half_sp + i].astype(F32) + peer_parts[i].astype(F32)
+        out[:, i * width : (i + 1) * width] = total.astype(BF16)
+
+
+def fused_device(n_sp, *args):
+    (tokens, norm_gain, query_down, query_gain, latent_down, latent_gain, rope_down, query_up,
+     key_up, value_up, glu_value, glu_gate, conv_taps, group_gain, head_proj, channel_proj) = args
+    rows, width = tokens.shape
+    depth, q_rank = query_down.shape
+    chans = glu_value.shape[1]
+    heads = key_up.shape[1] // NOPE
+    out_rows = head_proj.shape[0] + channel_proj.shape[0]
+    cols = head_proj.shape[1]
+    halo = (conv_taps.shape[0] // 2 + 15) // 16 * 16
+    tables = jnp.asarray(rope_tables(n_sp * rows))
+    vmem = pl.BlockSpec(memory_space=pltpu.VMEM)
+    hbm = pl.BlockSpec(memory_space=pl.ANY)
+    as_row = lambda v: v.reshape(1, -1)
+    operands = [
+        (tokens, hbm), (as_row(norm_gain), vmem), (query_down, hbm), (as_row(query_gain), vmem),
+        (latent_down, hbm), (as_row(latent_gain), vmem), (rope_down, hbm), (query_up, hbm),
+        (key_up, hbm), (value_up, hbm), (glu_value, hbm), (glu_gate, hbm), (conv_taps, vmem),
+        (as_row(group_gain), vmem), (head_proj, hbm), (channel_proj, hbm), (tables, hbm),
+    ]
+    like = lambda a: pltpu.VMEM(a.shape, a.dtype)
+    dma = pltpu.SemaphoreType.DMA
+    scratch = [
+        pltpu.VMEM((n_sp, depth, q_rank // 2), BF16),
+        pltpu.VMEM((n_sp, depth, 2 * chans), BF16),
+        pltpu.VMEM((n_sp, out_rows, cols), BF16),
+        like(tokens), like(latent_down), like(rope_down), like(query_up), like(key_up), like(value_up),
+        pltpu.VMEM((3, rows, LANES), F32),
+        pltpu.VMEM((rows, width), BF16),
+        pltpu.VMEM((n_sp, rows, KVR + LANES), BF16),
+        pltpu.VMEM((rows, LANES), F32),
+        pltpu.VMEM((rows, q_rank // 2), F32),
+        pltpu.VMEM((2, rows, q_rank // 2), F32),
+        pltpu.VMEM((rows, query_up.shape[1]), F32),
+        pltpu.VMEM((rows, 2 * chans), F32),
+        pltpu.VMEM((rows, out_rows), BF16),
+        pltpu.VMEM((rows, chans), BF16),
+        pltpu.VMEM((halo, chans), BF16),
+        pltpu.VMEM((halo, chans), BF16),
+        pltpu.VMEM((rows + 2 * halo, chans), F32),
+        pltpu.VMEM((n_sp, rows, cols), BF16),
+        pltpu.VMEM((n_sp // 2, rows, cols), BF16),
+        dma((12,)), dma((4, n_sp, 5)), dma((4, n_sp, 7)), dma((n_sp,)), dma((n_sp,)),
+        dma((2,)), dma((2,)), dma((2,)), dma((2,)),
+    ]
+    return pl.pallas_call(
+        functools.partial(fused_kernel, n_sp),
+        out_shape=(
+            jax.ShapeDtypeStruct((rows, n_sp * cols // 2), BF16),
+            jax.ShapeDtypeStruct((heads, rows), F32),
+        ),
+        in_specs=[spec for _, spec in operands],
+        out_specs=(vmem, vmem),
+        scratch_shapes=scratch,
+        compiler_params=pltpu.CompilerParams(
+            collective_id=0, has_side_effects=True, vmem_limit_bytes=48 * 1024 * 1024
+        ),
+        name="fused_layer",
+    )(*[value for value, _ in operands])
+
+
 def solution(mesh):
     in_specs = (
         P(("fs", "sp"), None),
@@ -191,6 +700,9 @@
         P("tp", "sp"),
     )
     out_specs = (P(("fs", "sp"), "tp"), P("tp", ("fs", "sp")))
+    body = per_device
+    if mesh.shape["fs"] == 4 and mesh.shape["tp"] == 2 and mesh.shape["sp"] in (2, 4):
+        body = functools.partial(fused_device, mesh.shape["sp"])
     return jax.shard_map(
-        per_device, mesh=mesh, in_specs=in_specs, out_specs=out_specs, check_vma=False
-    )
+        body, mesh=mesh, in_specs=in_specs, out_specs=out_specs, check_vma=False
+    )

time: 251 us -> 104 us (0.41)
  waiting for transfers between devices: 190 us -> 0 us
  Pallas kernels: 0 us -> 87.3 us
  blocking collectives: 17.5 us -> 0 us
  between operations: 14.7 us -> 0.68 us
  local copies, waits for them, and re-layouts: 2.34 us -> 15.3 us
  matrix products: 12.5 us -> 0 us
  other arithmetic: 9.21 us -> 0 us
  starting transfers between devices: 4.14 us -> 0 us
    all_gather x4 -> x0, waiting for transfers between devices: 182 us -> none  [the longest x1 72 us: per_device(): lax.all_gather(out_weight, 'sp', axis=1, tiled=True)]
    pallas_call x0 -> x1, Pallas kernels: none -> 87.3 us  [fused_device(): pl.pallas_call(functools.partial(fused_kernel, n_sp), out_shape=(jax.Shap...]
    all_gather x1 -> x0, blocking collectives: 17.5 us -> none  [per_device(): block_keys = lax.all_gather(own_keys, ('sp', 'tp'), axis=0, tiled=True)]
    dot_general x10 -> x0, matrix products: 12.5 us -> none  [the longest x1 3.71 us: per_device(): jnp.dot(mixed_in, lax.all_gather(out_weight, 'sp', axis=1, tiled=True), p...]
    unnamed x90 -> x25, local copies, waits for them, and re-layouts: 0.85 us -> 12.5 us
    reduce_scatter x1 -> x0, waiting for transfers between devices: 5.98 us -> none  [per_device(): lax.psum_scatter(partial_terms.astype(jnp.bfloat16), 'tp', scatter_dimens...]
    ppermute x2 -> x0, starting transfers between devices: 3.94 us -> none  [the longest x1 2.66 us: padded_2(): lax.ppermute(lax.slice_in_dim(block, block.shape[dim] - width, None, axis...]
    add x2 -> x0, other arithmetic: 2.92 us -> none  [the longest x1 2.33 us: per_device(): filtered + padded[tap_index:tap_index + tok_count].astype(jnp.float32) *...]
  transfers between devices with their start and end apart: 7 -> 0, of which waited for: 5 -> 0; matrix products, arithmetic and copies ran while one was open for 8% -> 0% of each run, Pallas kernels for 0% -> 0%
where the time goes in v1:
time: 104 us; the launch traced here: 103 us
  Pallas kernels  87.3 us (84%)
  local copies, waits for them, and re-layouts  15.3 us (15%)
    pallas_call x1, Pallas kernels, fused_device(): pl.pallas_call(functools.partial(fused_kernel, n_sp), out_shape=(jax.Shap...  87.3 us
    unnamed x25, local copies, waits for them, and re-layouts  12.5 us
    reshape x4, local copies, waits for them, and re-layouts, fused_device(): as_row = lambda v: v.reshape(1, -1)  2.79 us

profile of v1, /device:TPU:0, one launch (start us, length us, event | category | flops | bytes accessed | tf_op | source)
XLA Modules:
  0.0 103.3 jit_solution(18383343036492021742)
XLA Ops:
  0.6 0.0 copy-start
  0.6 0.7 reshape.18.latent_gain
  1.4 0.7 reshape.17.query_gain
  2.1 0.7 reshape.19.group_gain
  2.7 0.7 reshape.16.norm_gain
  3.4 1.2 %copy.19.rope_down = bf16[2048,64]{1,0:T(8,128)(2,1)S(1)} copy(bf16[2048,64]{0,1:T(8,128)(2,1)} %param.23) | data formatting | bytes 524288 | tf_op args[6]
  4.7 0.0 copy-done
  4.7 0.0 copy-start.1
  4.7 1.1 %copy-done.1 = f32[3,512,128]{2,1,0:T(8,128)S(1)} copy-done((f32[3,512,128]{2,1,0:T(8,128)S(1)}, f32[3,512,128]{2,1,0:T(8,128)}, u32[]{:S(2)}) %copy-start.1) | copy-done | bytes 786456
  5.8 0.0 copy-start.2
  5.8 1.0 %copy-done.2 = bf16[128,2048]{1,0:T(8,128)(2,1)S(1)} copy-done((bf16[128,2048]{1,0:T(8,128)(2,1)S(1)}, bf16[128,2048]{1,0:T(8,128)(2,1)}, u32[]{:S(2)}) %copy-start.2) | copy-done | bytes 524312
  6.8 0.0 copy-start.3
  6.8 1.0 %copy-done.3 = bf16[512,512]{1,0:T(8,128)(2,1)S(1)} copy-done((bf16[512,512]{1,0:T(8,128)(2,1)S(1)}, bf16[512,512]{1,0:T(8,128)(2,1)}, u32[]{:S(2)}) %copy-start.3) | copy-done | bytes 524312
  7.9 0.0 copy-start.4
  7.9 1.0 %copy-done.4 = bf16[512,512]{1,0:T(8,128)(2,1)S(1)} copy-done((bf16[512,512]{1,0:T(8,128)(2,1)S(1)}, bf16[512,512]{1,0:T(8,128)(2,1)}, u32[]{:S(2)}) %copy-start.4) | copy-done | bytes 524312
  8.9 0.0 copy-start.5
  8.9 1.0 %copy-done.5 = bf16[512,512]{1,0:T(8,128)(2,1)S(1)} copy-done((bf16[512,512]{1,0:T(8,128)(2,1)S(1)}, bf16[512,512]{1,0:T(8,128)(2,1)}, u32[]{:S(2)}) %copy-start.5) | copy-done | bytes 524312
  10.0 0.0 copy-start.6
  10.0 1.0 %copy-done.6 = bf16[512,512]{1,0:T(8,128)(2,1)S(1)} copy-done((bf16[512,512]{1,0:T(8,128)(2,1)S(1)}, bf16[512,512]{1,0:T(8,128)(2,1)}, u32[]{:S(2)}) %copy-start.6) | copy-done | bytes 524312
  11.0 0.0 copy-start.7
  11.0 1.0 %copy-done.7 = bf16[512,512]{1,0:T(8,128)(2,1)S(1)} copy-done((bf16[512,512]{1,0:T(8,128)(2,1)S(1)}, bf16[512,512]{1,0:T(8,128)(2,1)}, u32[]{:S(2)}) %copy-start.7) | copy-done | bytes 524312
  12.1 0.0 copy-start.8
  12.1 0.9 copy-done.8
  13.0 0.0 copy-start.9
  13.0 0.9 copy-done.9
  14.0 0.0 copy-start.10
  14.0 0.8 copy-done.10
  14.7 87.3 %fused_layer.1 = (bf16[128,1024]{1,0:T(8,128)(2,1)S(1)}, f32[4,128]{1,0:T(4,128)S(1)}) custom-call(bf16[128,2048]{1,0:T(8,128)(2,1)S(1)} %copy-done.2, bf16[1,2048]{1,0:T(2,128)(2,1)S(1)} %reshape.16.norm_gain, bf16[512,512]{1,0:T(8,128)(2,1)S(1)} %copy-done.3, bf16[1,512]{1,0:T(2,128)(2,1)S(1)} %reshape.17.query_gain, bf16[2048,256]{1,0:T(8,128)(2,1)} %latent_down.1, ...), custom_call_target="tpu_custom_call" | custom-call | tf_op jit(solution)/shard_map/fused_layer/pallas_call | solution.py:667
  102.0 0.7 copy.22
  102.8 0.6 copy.23
Async XLA Ops:
  0.6 4.0 %copy-start = (bf16[512,768]{1,0:T(8,128)(2,1)S(1)}, bf16[512,768]{1,0:T(8,128)(2,1)}, u32[]{:S(2)}) copy-start(bf16[512,768]{1,0:T(8,128)(2,1)} %query_up.1) | copy-start | bytes 2359300
  4.7 1.1 %copy-start.1 = (f32[3,512,128]{2,1,0:T(8,128)S(1)}, f32[3,512,128]{2,1,0:T(8,128)}, u32[]{:S(2)}) copy-start(f32[3,512,128]{2,1,0:T(8,128)} %constant.2.clone.tables) | copy-start | bytes 2359300
  5.8 1.0 %copy-start.2 = (bf16[128,2048]{1,0:T(8,128)(2,1)S(1)}, bf16[128,2048]{1,0:T(8,128)(2,1)}, u32[]{:S(2)}) copy-start(bf16[128,2048]{1,0:T(8,128)(2,1)} %tokens.1) | copy-start | bytes 1572868
  6.8 1.0 %copy-start.3 = (bf16[512,512]{1,0:T(8,128)(2,1)S(1)}, bf16[512,512]{1,0:T(8,128)(2,1)}, u32[]{:S(2)}) copy-start(bf16[512,512]{1,0:T(8,128)(2,1)} %query_down.1) | copy-start | bytes 1572868
  7.9 1.0 %copy-start.4 = (bf16[512,512]{1,0:T(8,128)(2,1)S(1)}, bf16[512,512]{1,0:T(8,128)(2,1)}, u32[]{:S(2)}) copy-start(bf16[512,512]{1,0:T(8,128)(2,1)} %glu_value.1) | copy-start | bytes 1572868
  8.9 1.0 %copy-start.5 = (bf16[512,512]{1,0:T(8,128)(2,1)S(1)}, bf16[512,512]{1,0:T(8,128)(2,1)}, u32[]{:S(2)}) copy-start(bf16[512,512]{1,0:T(8,128)(2,1)} %glu_gate.1) | copy-start | bytes 1572868
  10.0 1.0 %copy-start.6 = (bf16[512,512]{1,0:T(8,128)(2,1)S(1)}, bf16[512,512]{1,0:T(8,128)(2,1)}, u32[]{:S(2)}) copy-start(bf16[512,512]{1,0:T(8,128)(2,1)} %head_proj.1) | copy-start | bytes 1572868
  11.0 1.0 %copy-start.7 = (bf16[512,512]{1,0:T(8,128)(2,1)S(1)}, bf16[512,512]{1,0:T(8,128)(2,1)}, u32[]{:S(2)}) copy-start(bf16[512,512]{1,0:T(8,128)(2,1)} %channel_proj.1) | copy-start | bytes 1572868
  12.1 0.9 copy-start.8
  13.0 0.9 copy-start.9
  14.0 0.8 copy-start.10

commit v2 on v1

--- a/solution.py
+++ b/solution.py
@@ -205,6 +205,10 @@
     return jnp.dot(a, b, preferred_element_type=F32)
 
 
+def row_of(ref):
+    return ref[...].reshape(1, -1)
+
+
 def dot_nt(a, b):
     return lax.dot_general(a, b, (((1,), (1,)), ((), ())), preferred_element_type=F32)
 
@@ -214,10 +218,10 @@
     tokens, norm_gain, query_down, query_gain, latent_down, latent_gain, rope_down, query_up,
     key_up, value_up, glu_value, glu_gate, conv_taps, group_gain, head_proj, channel_proj, tables,
     out, log_out,
-    w_q, w_g, w_o, tok_v, lat_v, rope_v, qup_v, kup_v, vup_v, tab_v,
-    normed, keys, key_tmp, q_acc, q_lat, q_scr, g_acc, mixed, gated, low_rows, high_rows, padded,
+    w_q, w_v, w_t, w_o, tok_v, lat_v, rope_v, qup_v, kup_v, vup_v, tab_v,
+    normed, keys, key_tmp, q_acc, q_lat, q_scr, v_acc, t_acc, mixed, gated, low_rows, high_rows, padded,
     parts, peer_parts,
-    load_sem, recv_sem, send_sem, key_recv, key_send, pair_recv, pair_send, halo_recv, halo_send,
+    load_sem, recv_sem, send_sem, key_recv, key_send, key_pair_recv, key_pair_send, pair_recv, pair_send, halo_recv, halo_send,
 ):
     z = lax.axis_index("sp")
     c = lax.axis_index("fs")
@@ -242,8 +246,8 @@
         loads[name] = copy
 
     load("wq", query_down.at[:, pl.ds(pl.multiple_of(t * q_cols, LANES), q_cols)], w_q.at[z])
-    load("gv", glu_value, w_g.at[z, :, pl.ds(0, chans)])
-    load("gg", glu_gate, w_g.at[z, :, pl.ds(chans, chans)])
+    load("gv", glu_value, w_v.at[z])
+    load("gg", glu_gate, w_t.at[z])
     load("tok", tokens, tok_v)
     load("lat", latent_down, lat_v)
     load("rope", rope_down, rope_v)
@@ -255,20 +259,31 @@
     load("vup", value_up, vup_v)
 
     barrier = pltpu.get_barrier_semaphore()
-    partners = [{"sp": (z + d) % n_sp} for d in range(1, n_sp)]
-    partners += [{"fs": c_x}, {"fs": c_y}, {"tp": peer}]
-    for partner in partners:
+    sides = [{"fs": c_x}, {"fs": c_y}, {"tp": peer}]
+    for partner in sides:
         pl.semaphore_signal(barrier, inc=1, device_id=partner, device_id_type=MESH)
-    pl.semaphore_wait(barrier, len(partners))
+
+    @pl.when(z > 0)
+    def _():
+        pl.semaphore_signal(barrier, inc=1, device_id={"sp": z - 1}, device_id_type=MESH)
+
+    @pl.when(z < n_sp - 1)
+    def _():
+        pl.semaphore_signal(barrier, inc=1, device_id={"sp": z + 1}, device_id_type=MESH)
+
+    ends = (z == 0).astype(jnp.int32) + (z == n_sp - 1).astype(jnp.int32)
+    pl.semaphore_wait(barrier, len(sides) + 2 - ends)
 
     direct_rows = (out_rows // 4) // 64 * 64
     units = [
         (w_q, 0, depth, True),
-        (w_g, 0, depth, True),
-        (w_o, 0, out_rows - direct_rows, True),
+        (w_v, 0, depth, True),
+        (w_t, 0, depth, True),
+        (w_o, 0, head_rows, True),
+        (w_o, head_rows, out_rows - head_rows - direct_rows, True),
         (w_o, out_rows - direct_rows, direct_rows, False),
     ]
-    Q, G, O, D = range(4)
+    Q, V, T, H, P, D = range(6)
 
     def block(u, shard, quarter, half=None):
         buf, first, count, shared = units[u]
@@ -359,15 +374,13 @@
         wait_in(u, k, DY_IN, c_d, 0)
         wait_in(u, k, DX_IN, c_d, 1)
 
-    loads["wq"].wait()
-    send_own(Q)
-    loads["gv"].wait()
-    loads["gg"].wait()
-    send_own(G)
+    for name, u in (("wq", Q), ("gv", V), ("gg", T)):
+        loads[name].wait()
+        send_own(u)
 
     loads["tok"].wait()
     values = tok_v[...].astype(F32)
-    normed[...] = rms_scale(values, norm_gain[...]).astype(BF16)
+    normed[...] = rms_scale(values, row_of(norm_gain)).astype(BF16)
 
     def rotate_lanes(v):
         half = ROPE // 2
@@ -376,31 +389,49 @@
         )
 
     loads["lat"].wait()
-    latent = rms_scale(dot(normed[...], lat_v[...]), latent_gain[...])
+    latent = rms_scale(dot(normed[...], lat_v[...]), row_of(latent_gain))
     keys[z, :, 0:KVR] = latent.astype(BF16)
     loads["rope"].wait()
     loads["tab"].wait()
     key_tmp[...] = jnp.zeros_like(key_tmp)
-    key_tmp[:, 0:ROPE] = dot(normed[...], rope_v[...])
+    key_tmp[:, 0:ROPE] = dot_nt(normed[...], rope_v[...])
     keys[z, :, KVR : KVR + LANES] = rotate_lanes(key_tmp[...]).astype(BF16)
 
-    def key_copy(d):
+    half_rows = rows // 2
+
+    def key_half(shard, half):
+        return keys.at[shard, pl.ds(pl.multiple_of(half * half_rows, 16), half_rows), :]
+
+    def key_copy(shard, kind, target):
         return pltpu.make_async_remote_copy(
-            src_ref=keys.at[z], dst_ref=keys.at[z],
-            send_sem=key_send.at[d], recv_sem=key_recv.at[d],
-            device_id={"sp": (z + d) % n_sp}, device_id_type=MESH,
+            src_ref=key_half(shard, t), dst_ref=key_half(shard, t),
+            send_sem=key_send.at[shard, kind], recv_sem=key_recv.at[shard],
+            device_id={"sp": target}, device_id_type=MESH,
         )
 
-    def key_arrival(d):
-        source = (z + n_sp - d) % n_sp
+    def key_pair(shard, half):
         return pltpu.make_async_remote_copy(
-            src_ref=keys.at[source], dst_ref=keys.at[source],
-            send_sem=key_send.at[d], recv_sem=key_recv.at[d],
-            device_id={"sp": source}, device_id_type=MESH,
+            src_ref=key_half(shard, half), dst_ref=key_half(shard, half),
+            send_sem=key_pair_send.at[shard], recv_sem=key_pair_recv.at[shard],
+            device_id={"tp": peer}, device_id_type=MESH,
         )
 
-    for d in range(1, n_sp):
-        key_copy(d).start()
+    def own_keys(action):
+        @pl.when(z > 0)
+        def _():
+            action(key_copy(z, Z_LOW, z - 1))
+
+        @pl.when(z < n_sp - 1)
+        def _():
+            action(key_copy(z, Z_HIGH, z + 1))
+
+    own_keys(lambda copy: copy.start())
+
+    def step_k(k):
+        shard, target = arrivals[k]
+        key_copy(shard, Z_FWD, target).wait_recv()
+        when_forward(k, lambda: key_copy(shard, Z_FWD, target).start())
+        key_pair(shard, t).start()
 
     def add_shard(acc, weights, shard, first=False):
         columns = pl.ds(pl.multiple_of(shard * depth, LANES), depth)
@@ -408,24 +439,39 @@
         acc[...] = term if first else acc[...] + term
 
     add_shard(q_acc, w_q, z, True)
-    add_shard(g_acc, w_g, z, True)
+    add_shard(v_acc, w_v, z, True)
+    add_shard(t_acc, w_t, z, True)
+    accs = {Q: (q_acc, w_q), V: (v_acc, w_v), T: (t_acc, w_t)}
+
+    def step_cm(u, k):
+        step_c(u, k)
+        add_shard(*accs[u], arrivals[k][0])
 
     last = n_sp - 2
     loads["hp"].wait()
     loads["cp"].wait()
     for k in range(last + 1):
-        step_a(Q, k)
-        if k:
-            step_b(Q, k - 1)
-        if k > 1:
-            step_c(Q, k - 2)
-            add_shard(q_acc, w_q, arrivals[k - 2][0])
-    send_own(O)
-    step_b(Q, last)
-    step_a(G, 0)
-    for k in range(max(last - 1, 0), last + 1):
-        step_c(Q, k)
-        add_shard(q_acc, w_q, arrivals[k][0])
+        for u in (Q, V, T):
+            step_a(u, k)
+            if k:
+                step_b(u, k - 1)
+            if k > 1:
+                step_cm(u, k - 2)
+        step_k(k)
+        if k == 1:
+            send_own(H)
+    send_own(P)
+    step_a(H, 0)
+    for u in (Q, V, T):
+        step_b(u, last)
+    step_a(H, 1)
+    send_own(D)
+    for u in (Q, V, T):
+        step_cm(u, last - 1)
+    step_a(H, 2)
+    step_a(P, 0)
+    step_b(H, 0)
+    step_cm(Q, last)
 
     q_lat[t] = q_acc[...]
     q_copy = pltpu.make_async_remote_copy(
@@ -441,10 +487,10 @@
         recv_sem=pair_recv.at[0], device_id={"tp": peer}, device_id_type=MESH,
     ).wait_recv()
     whole_q = jnp.concatenate([q_lat[0], q_lat[1]], axis=1)
-    latent_query = rms_scale(whole_q, query_gain[...]).astype(BF16)
+    latent_query = rms_scale(whole_q, row_of(query_gain)).astype(BF16)
     q_scr[...] = dot(latent_query, qup_v[...])
-    for d in range(1, n_sp):
-        key_arrival(d).wait_recv()
+    for k in range(n_sp - 1):
+        key_pair(arrivals[k][0], peer).wait_recv()
 
     def attend(h, shifted):
         start = h * (NOPE + ROPE)
@@ -470,37 +516,21 @@
     shifted = pltpu.roll(whole, whole.shape[1] - ROPE, 1)
     lane = lax.broadcasted_iota(jnp.int32, (rows, LANES), 1)
     logs = jnp.zeros((rows, LANES), F32)
-    relays = [lambda: step_a(G, 1), lambda: step_b(G, 0), lambda: step_a(G, 2), lambda: None]
-    if n_sp == 2:
-        relays = [lambda: step_b(G, 0)]
+    relays = [
+        lambda: step_a(P, 1), lambda: step_b(H, 1), lambda: (step_a(D, 0), step_a(P, 2)),
+        lambda: step_b(P, 0),
+    ]
     for h in range(heads):
         logs = jnp.where(lane == h, attend(h, shifted), logs)
-        if h < len(relays):
-            relays[h]()
-    for h in range(heads, len(relays)):
         relays[h]()
     log_out[...] = jnp.transpose(logs)[0:heads, :]
 
-    send_own(D)
-    if n_sp > 2:
-        step_b(G, 1)
-        step_c(G, 0)
-        add_shard(g_acc, w_g, arrivals[0][0])
-        step_a(O, 0)
-        step_b(G, 2)
-        step_c(G, 1)
-        add_shard(g_acc, w_g, arrivals[1][0])
-        step_a(O, 1)
-        step_c(G, 2)
-        add_shard(g_acc, w_g, arrivals[2][0])
-    else:
-        step_a(O, 0)
-        step_c(G, 0)
-        add_shard(g_acc, w_g, arrivals[0][0])
+    step_cm(V, last)
+    step_cm(T, last)
 
     halo = low_rows.shape[0]
     reach = conv_taps.shape[0] // 2
-    gated[...] = (g_acc[:, 0:chans] * jax.nn.sigmoid(g_acc[:, chans : 2 * chans])).astype(BF16)
+    gated[...] = (v_acc[...] * jax.nn.sigmoid(t_acc[...])).astype(BF16)
     up_copy = pltpu.make_async_remote_copy(
         src_ref=gated.at[pl.ds(rows - halo, halo), :], dst_ref=low_rows,
         send_sem=halo_send.at[0], recv_sem=halo_recv.at[0],
@@ -521,9 +551,8 @@
         down_copy.start()
 
     padded[halo : halo + rows, :] = gated[...].astype(F32)
-    step_b(O, 0)
-    if n_sp > 2:
-        step_a(O, 2)
+    step_a(D, 1)
+    step_b(H, 2)
 
     @pl.when(z > 0)
     def _():
@@ -544,6 +573,10 @@
         padded[halo + rows : 2 * halo + rows, :] = jnp.zeros((halo, chans), F32)
 
     group = CH // GROUPS
+    gains = row_of(group_gain).astype(F32)
+    between = [
+        lambda: step_b(P, 1), lambda: step_c(H, 0), lambda: step_a(D, 2), lambda: step_b(P, 2),
+    ]
     for g in range(chans // group):
         lanes = slice(g * group, (g + 1) * group)
         taps = conv_taps[:, lanes].astype(F32)
@@ -553,30 +586,20 @@
             filtered = filtered + padded[first : first + rows, lanes] * taps[j : j + 1, :]
         centred = filtered - jnp.mean(filtered, axis=1, keepdims=True)
         spread = jnp.mean(centred * centred, axis=1, keepdims=True)
-        branch = centred * lax.rsqrt(spread + norm_eps) * group_gain[:, lanes].astype(F32)
+        branch = centred * lax.rsqrt(spread + norm_eps) * gains[:, lanes]
         branch = branch * jax.nn.sigmoid(branch)
         mixed[:, heads * VDIM + g * group : heads * VDIM + (g + 1) * group] = branch.astype(BF16)
-        if g == 0 and n_sp > 2:
-            step_b(O, 1)
-        if g == 2:
-            step_c(O, 0)
-            step_a(D, 0)
+        between[g]()
 
     def add_part(shard):
         parts[shard] = dot(mixed[...], w_o[shard]).astype(BF16)
 
     add_part(z)
-    if n_sp > 2:
-        step_a(D, 1)
-        add_part(arrivals[0][0])
-        step_b(O, 2)
-        step_c(O, 1)
-        step_a(D, 2)
-        add_part(arrivals[1][0])
-        step_c(O, 2)
-        add_part(arrivals[2][0])
-    else:
-        add_part(arrivals[0][0])
+    for k in range(n_sp - 1):
+        if k:
+            step_c(H, k)
+        step_c(P, k)
+        add_part(arrivals[k][0])
 
     half_sp = n_sp // 2
     p_copy = pltpu.make_async_remote_copy(
@@ -600,8 +623,11 @@
             if units[u][3]:
                 for copy in side_copies(u, k) + corner_copies(u, k):
                     copy.wait_send()
-    for d in range(1, n_sp):
-        key_copy(d).wait_send()
+    own_keys(lambda copy: copy.wait_send())
+    for k in range(n_sp - 1):
+        shard, target = arrivals[k]
+        when_forward(k, lambda: key_copy(shard, Z_FWD, target).wait_send())
+        key_pair(shard, t).wait_send()
     q_copy.wait_send()
 
     @pl.when(z < n_sp - 1)
@@ -631,11 +657,11 @@
     halo = (conv_taps.shape[0] // 2 + 15) // 16 * 16
     tables = jnp.asarray(rope_tables(n_sp * rows))
     vmem = pl.BlockSpec(memory_space=pltpu.VMEM)
-    hbm = pl.BlockSpec(memory_space=pl.ANY)
-    as_row = lambda v: v.reshape(1, -1)
+    hbm = pl.BlockSpec(memory_space=pltpu.HBM)
+    as_row = lambda v: v
     operands = [
         (tokens, hbm), (as_row(norm_gain), vmem), (query_down, hbm), (as_row(query_gain), vmem),
-        (latent_down, hbm), (as_row(latent_gain), vmem), (rope_down, hbm), (query_up, hbm),
+        (latent_down, hbm), (as_row(latent_gain), vmem), (rope_down.T, hbm), (query_up, hbm),
         (key_up, hbm), (value_up, hbm), (glu_value, hbm), (glu_gate, hbm), (conv_taps, vmem),
         (as_row(group_gain), vmem), (head_proj, hbm), (channel_proj, hbm), (tables, hbm),
     ]
@@ -643,9 +669,10 @@
     dma = pltpu.SemaphoreType.DMA
     scratch = [
         pltpu.VMEM((n_sp, depth, q_rank // 2), BF16),
-        pltpu.VMEM((n_sp, depth, 2 * chans), BF16),
+        pltpu.VMEM((n_sp, depth, chans), BF16),
+        pltpu.VMEM((n_sp, depth, chans), BF16),
         pltpu.VMEM((n_sp, out_rows, cols), BF16),
-        like(tokens), like(latent_down), like(rope_down), like(query_up), like(key_up), like(value_up),
+        like(tokens), like(latent_down), pltpu.VMEM(rope_down.shape[::-1], BF16), like(query_up), like(key_up), like(value_up),
         pltpu.VMEM((3, rows, LANES), F32),
         pltpu.VMEM((rows, width), BF16),
         pltpu.VMEM((n_sp, rows, KVR + LANES), BF16),
@@ -653,7 +680,8 @@
         pltpu.VMEM((rows, q_rank // 2), F32),
         pltpu.VMEM((2, rows, q_rank // 2), F32),
         pltpu.VMEM((rows, query_up.shape[1]), F32),
-        pltpu.VMEM((rows, 2 * chans), F32),
+        pltpu.VMEM((rows, chans), F32),
+        pltpu.VMEM((rows, chans), F32),
         pltpu.VMEM((rows, out_rows), BF16),
         pltpu.VMEM((rows, chans), BF16),
         pltpu.VMEM((halo, chans), BF16),
@@ -661,7 +689,8 @@
         pltpu.VMEM((rows + 2 * halo, chans), F32),
         pltpu.VMEM((n_sp, rows, cols), BF16),
         pltpu.VMEM((n_sp // 2, rows, cols), BF16),
-        dma((12,)), dma((4, n_sp, 5)), dma((4, n_sp, 7)), dma((n_sp,)), dma((n_sp,)),
+        dma((12,)), dma((6, n_sp, 5)), dma((6, n_sp, 7)), dma((n_sp,)), dma((n_sp, 3)), dma((n_sp,)),
+        dma((n_sp,)),
         dma((2,)), dma((2,)), dma((2,)), dma((2,)),
     ]
     return pl.pallas_call(
@@ -674,7 +703,7 @@
         out_specs=(vmem, vmem),
         scratch_shapes=scratch,
         compiler_params=pltpu.CompilerParams(
-            collective_id=0, has_side_effects=True, vmem_limit_bytes=48 * 1024 * 1024
+            collective_id=0, has_side_effects=True, vmem_limit_bytes=63 * 1024 * 1024
         ),
         name="fused_layer",
     )(*[value for value, _ in operands])
@@ -701,7 +730,7 @@
     )
     out_specs = (P(("fs", "sp"), "tp"), P("tp", ("fs", "sp")))
     body = per_device
-    if mesh.shape["fs"] == 4 and mesh.shape["tp"] == 2 and mesh.shape["sp"] in (2, 4):
+    if mesh.shape["fs"] == 4 and mesh.shape["tp"] == 2 and mesh.shape["sp"] == 4:
         body = functools.partial(fused_device, mesh.shape["sp"])
     return jax.shard_map(
         body, mesh=mesh, in_specs=in_specs, out_specs=out_specs, check_vma=False

time: 104 us -> 78.7 us (0.76)
  local copies, waits for them, and re-layouts: 15.3 us -> 2.25 us
  Pallas kernels: 87.3 us -> 75.6 us
    pallas_call x1, Pallas kernels: 87.3 us -> 75.6 us  [fused_device(): pl.pallas_call(functools.partial(fused_kernel, n_sp), out_shape=(jax.Shap...]
    unnamed x25 -> x4, local copies, waits for them, and re-layouts: 12.5 us -> 2.25 us
    reshape x4 -> x0, local copies, waits for them, and re-layouts: 2.79 us -> none  [fused_device(): as_row = lambda v: v.reshape(1, -1)]
where the time goes in v2:
time: 78.7 us; the launch traced here: 78.5 us
  Pallas kernels  75.6 us (96%)
  local copies, waits for them, and re-layouts  2.25 us (3%)
    pallas_call x1, Pallas kernels, fused_device(): pl.pallas_call(functools.partial(fused_kernel, n_sp), out_shape=(jax.Shap...  75.6 us
    unnamed x4, local copies, waits for them, and re-layouts  2.25 us

profile of v2, /device:TPU:0, one launch (start us, length us, event | category | flops | bytes accessed | tf_op | source)
XLA Modules:
  0.0 78.5 jit_solution(7859597067769957677)
XLA Ops:
  0.6 75.6 %fused_layer.1 = (bf16[128,1024]{1,0:T(8,128)(2,1)}, f32[4,128]{1,0:T(4,128)}) custom-call(bf16[128,2048]{1,0:T(8,128)(2,1)} %tokens.1, bf16[2048]{0:T(1024)(128)(2,1)} %norm_gain.1, bf16[512,512]{1,0:T(8,128)(2,1)} %query_down.1, bf16[512]{0:T(512)(128)(2,1)} %query_gain.1, bf16[2048,256]{1,0:T(8,128)(2,1)} %latent_down.1, bf16[256]{0:T(256)(128)(2,1)} %latent_gain.1, ...), custom_call_target="tpu_custom_call" | custom-call | tf_op jit(solution)/shard_map/fused_layer/pallas_call | solution.py:696
  76.2 0.0 copy-start
  76.2 1.7 %copy.21 = bf16[128,1024]{1,0:T(8,128)(2,1)} copy(bf16[128,1024]{1,0:T(8,128)(2,1)} %get-tuple-element.4) | data formatting | bytes 524288
  77.9 0.0 copy-done
  77.9 0.6 copy.22
Async XLA Ops:
  76.2 1.7 %copy-start = (f32[4,128]{1,0:T(4,128)S(1)}, f32[4,128]{1,0:T(4,128)}, u32[]{:S(2)}) copy-start(f32[4,128]{1,0:T(4,128)} %get-tuple-element.5) | copy-start | bytes 6148

commit v3 on v2

--- a/solution.py
+++ b/solution.py
@@ -274,7 +274,7 @@
     ends = (z == 0).astype(jnp.int32) + (z == n_sp - 1).astype(jnp.int32)
     pl.semaphore_wait(barrier, len(sides) + 2 - ends)
 
-    direct_rows = (out_rows // 4) // 64 * 64
+    direct_rows = (out_rows // 8) // 64 * 64
     units = [
         (w_q, 0, depth, True),
         (w_v, 0, depth, True),
@@ -461,17 +461,18 @@
         if k == 1:
             send_own(H)
     send_own(P)
+    step_b(Q, last)
     step_a(H, 0)
-    for u in (Q, V, T):
-        step_b(u, last)
+    step_b(V, last)
     step_a(H, 1)
+    step_b(T, last)
     send_own(D)
     for u in (Q, V, T):
         step_cm(u, last - 1)
+    step_b(H, 0)
+    step_a(P, 0)
+    step_cm(Q, last)
     step_a(H, 2)
-    step_a(P, 0)
-    step_b(H, 0)
-    step_cm(Q, last)
 
     q_lat[t] = q_acc[...]
     q_copy = pltpu.make_async_remote_copy(

time: 78.7 us -> 76.7 us (0.975)
  Pallas kernels: 75.6 us -> 73.6 us
    pallas_call x1, Pallas kernels: 75.6 us -> 73.6 us  [fused_device(): pl.pallas_call(functools.partial(fused_kernel, n_sp), out_shape=(jax.Shap...]
where the time goes in v3:
time: 76.7 us; the launch traced here: 76.5 us
  Pallas kernels  73.6 us (96%)
  local copies, waits for them, and re-layouts  2.25 us (3%)
    pallas_call x1, Pallas kernels, fused_device(): pl.pallas_call(functools.partial(fused_kernel, n_sp), out_shape=(jax.Shap...  73.6 us
    unnamed x4, local copies, waits for them, and re-layouts  2.25 us

profile of v3, /device:TPU:0, one launch (start us, length us, event | category | flops | bytes accessed | tf_op | source)
XLA Modules:
  0.0 76.5 jit_solution(9966188831781617378)
XLA Ops:
  0.6 73.6 %fused_layer.1 = (bf16[128,1024]{1,0:T(8,128)(2,1)}, f32[4,128]{1,0:T(4,128)}) custom-call(bf16[128,2048]{1,0:T(8,128)(2,1)} %tokens.1, bf16[2048]{0:T(1024)(128)(2,1)} %norm_gain.1, bf16[512,512]{1,0:T(8,128)(2,1)} %query_down.1, bf16[512]{0:T(512)(128)(2,1)} %query_gain.1, bf16[2048,256]{1,0:T(8,128)(2,1)} %latent_down.1, bf16[256]{0:T(256)(128)(2,1)} %latent_gain.1, ...), custom_call_target="tpu_custom_call" | custom-call | tf_op jit(solution)/shard_map/fused_layer/pallas_call | solution.py:697
  74.3 0.0 copy-start
  74.3 1.7 %copy.21 = bf16[128,1024]{1,0:T(8,128)(2,1)} copy(bf16[128,1024]{1,0:T(8,128)(2,1)} %get-tuple-element.4) | data formatting | bytes 524288
  75.9 0.0 copy-done
  75.9 0.6 copy.22
Async XLA Ops:
  74.3 1.7 %copy-start = (f32[4,128]{1,0:T(4,128)S(1)}, f32[4,128]{1,0:T(4,128)}, u32[]{:S(2)}) copy-start(f32[4,128]{1,0:T(4,128)} %get-tuple-element.5) | copy-start | bytes 6148

commit v4 on v3

--- a/solution.py
+++ b/solution.py
@@ -592,23 +592,30 @@
         mixed[:, heads * VDIM + g * group : heads * VDIM + (g + 1) * group] = branch.astype(BF16)
         between[g]()
 
-    def add_part(shard):
-        parts[shard] = dot(mixed[...], w_o[shard]).astype(BF16)
-
-    add_part(z)
+    half_sp = n_sp // 2
+
+    def p_copy(i):
+        return pltpu.make_async_remote_copy(
+            src_ref=parts.at[peer * half_sp + i], dst_ref=peer_parts.at[i],
+            send_sem=pair_send.at[1 + i], recv_sem=pair_recv.at[1 + i],
+            device_id={"tp": peer}, device_id_type=MESH,
+        )
+
+    def add_part(shard, between_halves):
+        part = dot(mixed[:, 0:head_rows], w_o[shard, 0:head_rows, :])
+        between_halves()
+        part = part + dot(mixed[:, head_rows:out_rows], w_o[shard, head_rows:out_rows, :])
+        parts[shard] = part.astype(BF16)
+        for i in range(half_sp):
+            @pl.when(shard == peer * half_sp + i)
+            def _():
+                p_copy(i).start()
+
+    add_part(z, lambda: None)
     for k in range(n_sp - 1):
         if k:
             step_c(H, k)
-        step_c(P, k)
-        add_part(arrivals[k][0])
-
-    half_sp = n_sp // 2
-    p_copy = pltpu.make_async_remote_copy(
-        src_ref=parts.at[pl.ds(peer * half_sp, half_sp)], dst_ref=peer_parts,
-        send_sem=pair_send.at[1], recv_sem=pair_recv.at[1],
-        device_id={"tp": peer}, device_id_type=MESH,
-    )
-    p_copy.start()
+        add_part(arrivals[k][0], functools.partial(step_c, P, k))
 
     for u in range(len(units)):
         @pl.when(z > 0)
@@ -639,7 +646,8 @@
     def _():
         down_copy.wait_send()
 
-    p_copy.wait()
+    for i in range(half_sp):
+        p_copy(i).wait()
     width = parts.shape[2]
     for i in range(half_sp):
         total = parts[t * half_sp + i].astype(F32) + peer_parts[i].astype(F32)
@@ -692,7 +700,7 @@
         pltpu.VMEM((n_sp // 2, rows, cols), BF16),
         dma((12,)), dma((6, n_sp, 5)), dma((6, n_sp, 7)), dma((n_sp,)), dma((n_sp, 3)), dma((n_sp,)),
         dma((n_sp,)),
-        dma((2,)), dma((2,)), dma((2,)), dma((2,)),
+        dma((1 + n_sp // 2,)), dma((1 + n_sp // 2,)), dma((2,)), dma((2,)),
     ]
     return pl.pallas_call(
         functools.partial(fused_kernel, n_sp),

time: 76.7 us -> 76.6 us (level)
  no operation moved by 1% of the time
where the time goes in v4:
time: 76.6 us; the launch traced here: 76.4 us
  Pallas kernels  73.5 us (96%)
  local copies, waits for them, and re-layouts  2.25 us (3%)
    pallas_call x1, Pallas kernels, fused_device(): pl.pallas_call(functools.partial(fused_kernel, n_sp), out_shape=(jax.Shap...  73.5 us
    unnamed x4, local copies, waits for them, and re-layouts  2.25 us

profile of v4, /device:TPU:0, one launch (start us, length us, event | category | flops | bytes accessed | tf_op | source)
XLA Modules:
  0.0 76.4 jit_solution(15837005994373048394)
XLA Ops:
  0.6 73.5 %fused_layer.1 = (bf16[128,1024]{1,0:T(8,128)(2,1)}, f32[4,128]{1,0:T(4,128)}) custom-call(bf16[128,2048]{1,0:T(8,128)(2,1)} %tokens.1, bf16[2048]{0:T(1024)(128)(2,1)} %norm_gain.1, bf16[512,512]{1,0:T(8,128)(2,1)} %query_down.1, bf16[512]{0:T(512)(128)(2,1)} %query_gain.1, bf16[2048,256]{1,0:T(8,128)(2,1)} %latent_down.1, bf16[256]{0:T(256)(128)(2,1)} %latent_gain.1, ...), custom_call_target="tpu_custom_call" | custom-call | tf_op jit(solution)/shard_map/fused_layer/pallas_call | solution.py:705
  74.1 0.0 copy-start
  74.1 1.7 %copy.21 = bf16[128,1024]{1,0:T(8,128)(2,1)} copy(bf16[128,1024]{1,0:T(8,128)(2,1)} %get-tuple-element.4) | data formatting | bytes 524288
  75.8 0.0 copy-done
  75.8 0.6 copy.22
Async XLA Ops:
  74.1 1.7 %copy-start = (f32[4,128]{1,0:T(4,128)S(1)}, f32[4,128]{1,0:T(4,128)}, u32[]{:S(2)}) copy-start(f32[4,128]{1,0:T(4,128)} %get-tuple-element.5) | copy-start | bytes 6148
